TPU v7x, 32 devices: a whole 2x2x4 slice. The times are simulated.
32 devices in a mesh: ep: 16 (over z, y, x), tp: 2 (over core).
Axes of the slice: x: 2, y: 2, z: 4, core: 2. Of those that a mesh axis runs over, the one named last changes fastest.
Arguments:
- tokens: bfloat16 [256, 2048], P('ep'), may hold values from -6 to 6
- norm_attn: float32 [2048], replicated, may hold values from 0.1 to 1.9
- w_query: bfloat16 [2048, 2048], P(None, 'tp'), may hold values from -0.125 to 0.125
- w_key: bfloat16 [2048, 256], P(None, 'tp'), may hold values from -0.125 to 0.125
- w_value: bfloat16 [2048, 256], P(None, 'tp'), may hold values from -0.125 to 0.125
- w_out: bfloat16 [2048, 2048], P('tp'), may hold values from -0.125 to 0.125
- attn_bias: float32 [32], P('tp'), may hold values from -7 to -1
- cache_keys: bfloat16 [256, 1024, 256], P('ep', None, 'tp'), may hold values from -6 to 6
- cache_values: bfloat16 [256, 1024, 256], P('ep', None, 'tp'), may hold values from -6 to 6
- lengths: int32 [256], P('ep'), may hold values from 256 to 1024
- norm_ffn: float32 [2048], replicated, may hold values from 0.1 to 1.9
- expert_gate: bfloat16 [2048, 57344], P(None, ('ep', 'tp')), may hold values from -0.125 to 0.125
- expert_up: bfloat16 [2048, 57344], P(None, ('ep', 'tp')), may hold values from -0.125 to 0.125
- expert_down: bfloat16 [57344, 2048], P(('ep', 'tp')), may hold values from -0.0625 to 0.0625
- dense_gate_w: bfloat16 [2048, 7168], P(None, 'ep'), may hold values from -0.125 to 0.125
- dense_up_w: bfloat16 [2048, 7168], P(None, 'ep'), may hold values from -0.125 to 0.125
- dense_down_w: bfloat16 [7168, 2048], P('ep'), may hold values from -0.0625 to 0.0625
- dense_mix: bfloat16 [2048], replicated, may hold values from -0.125 to 0.125
- routes: int32 [256, 2], P(('ep', 'tp')), may hold values from 0 to 7, all different within a row; in each aligned block of 8 rows (0 to 7, 8 to 15, ...) at most 3 rows name the same one
- route_weights: bfloat16 [256, 2], P(('ep', 'tp')), may hold values from 0.19921875 to 1
Outputs:
- layer_out: bfloat16 [256, 2048], P(('ep', 'tp'))
- new_keys: bfloat16 [256, 256], P('ep', 'tp')
- new_values: bfloat16 [256, 256], P('ep', 'tp')
Inputs may be any that keep to these rules, and one draw needn't show every extreme that they name: `routes`: in each aligned block of 8 rows (the rows of one device) no expert is named by more than 3 rows, a bound that some block reaches; a row names 2 different experts.
All inputs are finite; a program needn't handle non-finite values.
Results may differ from a plain program's by a relative error of at most 0.015.
Values may be sent and summed in bfloat16 or wider, within the bound.
A program may use at most 128 MiB of HBM per device.

v0:
```python
import jax
import jax.numpy as jnp
from jax import lax
from jax.sharding import PartitionSpec as P

HEAD_DIM = 64
EXPERTS = 8
TOP = 2


EPSILON = 1e-06


def normed_rows(values, gain):
    widened = values.astype(jnp.float32)
    scale = lax.rsqrt(jnp.mean(widened * widened, axis=-1, keepdims=True) + EPSILON)
    return (widened * scale * gain).astype(jnp.bfloat16)


def later_sums(log_keep):
    cache_len = log_keep.shape[-1]
    block_len = 128
    block_count = cache_len // block_len
    lead = log_keep.shape[:-1]
    blocked = log_keep.reshape(lead + (block_count, block_len))
    rows_in = lax.broadcasted_iota(jnp.int32, (block_len, block_len), 0)
    cols_in = lax.broadcasted_iota(jnp.int32, (block_len, block_len), 1)
    upper = (rows_in >= cols_in).astype(jnp.float32)
    within = jnp.einsum("...nj,ji->...ni", blocked, upper, precision=lax.Precision.HIGHEST)
    totals = within[..., 0]
    rows_out = lax.broadcasted_iota(jnp.int32, (block_count, block_count), 0)
    cols_out = lax.broadcasted_iota(jnp.int32, (block_count, block_count), 1)
    beyond = (rows_out > cols_out).astype(jnp.float32)
    following = jnp.einsum("...m,mn->...n", totals, beyond, precision=lax.Precision.HIGHEST)
    inclusive = within + following[..., None]
    return (inclusive - blocked).reshape(log_keep.shape)


def running_ranks(present):
    count = present.shape[-1]
    rows_in = lax.broadcasted_iota(jnp.int32, (count, count), 0)
    cols_in = lax.broadcasted_iota(jnp.int32, (count, count), 1)
    lower = (rows_in <= cols_in).astype(jnp.float32)
    totals = jnp.einsum(
        "...j,ji->...i", present.astype(jnp.float32), lower, precision=lax.Precision.HIGHEST
    )
    return totals.astype(jnp.int32) - 1


def shards(
    tokens,
    norm_attn,
    w_query,
    w_key,
    w_value,
    w_out,
    attn_bias,
    cache_keys,
    cache_values,
    lengths,
    norm_ffn,
    expert_gate,
    expert_up,
    expert_down,
    dense_gate_w,
    dense_up_w,
    dense_down_w,
    dense_mix,
    routes,
    route_weights,
):
    seq_count = tokens.shape[0]
    cache_len = cache_keys.shape[1]
    group_count = cache_keys.shape[2] // HEAD_DIM
    repeat = w_query.shape[1] // (group_count * HEAD_DIM)
    normed = normed_rows(tokens, norm_attn)
    query = jnp.dot(normed, w_query, preferred_element_type=jnp.float32).astype(jnp.bfloat16)
    new_keys = jnp.dot(normed, w_key, preferred_element_type=jnp.float32).astype(jnp.bfloat16)
    new_values = jnp.dot(normed, w_value, preferred_element_type=jnp.float32).astype(jnp.bfloat16)
    query_heads = query.reshape(seq_count, group_count, repeat, HEAD_DIM)
    key_heads = cache_keys.reshape(seq_count, cache_len, group_count, HEAD_DIM)
    value_heads = cache_values.reshape(seq_count, cache_len, group_count, HEAD_DIM)
    scores = jnp.einsum(
        "bgrd,bsgd->bgrs", query_heads, key_heads, preferred_element_type=jnp.float32
    ) * HEAD_DIM ** (-0.5)
    scores = scores + attn_bias.reshape(group_count, repeat)[None, :, :, None]
    places = lax.broadcasted_iota(jnp.int32, (seq_count, cache_len), 1)
    visible = (places < lengths[:, None])[:, None, None, :]
    log_keep = jnp.where(visible, jax.nn.log_sigmoid(-scores), 0.0)
    after = later_sums(log_keep)
    weight = jnp.where(visible, jnp.exp(jax.nn.log_sigmoid(scores) + after), 0.0).astype(
        jnp.bfloat16
    )
    heads_out = jnp.einsum(
        "bgrs,bsgd->bgrd", weight, value_heads, preferred_element_type=jnp.float32
    )
    heads_out = heads_out.astype(jnp.bfloat16).reshape(seq_count, group_count * repeat * HEAD_DIM)
    partial_value = jnp.dot(heads_out, w_out, preferred_element_type=jnp.float32)
    attn_sum = lax.psum_scatter(
        partial_value.astype(jnp.bfloat16), "tp", scatter_dimension=0, tiled=True
    ).astype(jnp.float32)
    row_count = seq_count // lax.axis_size("tp")
    capacity = (row_count * TOP + EXPERTS - 1) // EXPERTS + 1
    own_rows = lax.dynamic_slice_in_dim(tokens, lax.axis_index("tp") * row_count, row_count, 0)
    middle = (own_rows.astype(jnp.float32) + attn_sum).astype(jnp.bfloat16)
    normed_two = normed_rows(middle, norm_ffn)
    width = normed_two.shape[1]
    piece = lax.all_gather(normed_two, "ep", axis=0, tiled=True)
    mix_gate = jax.nn.sigmoid(jnp.dot(piece, dense_mix, preferred_element_type=jnp.float32))
    dense_hidden = (
        jax.nn.silu(jnp.dot(piece, dense_gate_w, preferred_element_type=jnp.float32))
        * jnp.dot(piece, dense_up_w, preferred_element_type=jnp.float32)
    ).astype(jnp.bfloat16)
    dense_terms = (
        jnp.dot(dense_hidden, dense_down_w, preferred_element_type=jnp.float32) * mix_gate[:, None]
    )
    dense_term = lax.psum_scatter(dense_terms, "ep", scatter_dimension=0, tiled=True)
    devices = lax.axis_size(("ep", "tp"))
    members = devices // EXPERTS
    expert_ids = lax.broadcasted_iota(jnp.int32, (EXPERTS, 1, 1), 0)
    matched = routes[None, :, :] == expert_ids
    present = jnp.any(matched, axis=2).astype(jnp.int32)
    share = jnp.sum(jnp.where(matched, route_weights.astype(jnp.float32)[None, :, :], 0.0), axis=2)
    ranks = running_ranks(present)
    slot_ids = lax.broadcasted_iota(jnp.int32, (EXPERTS, capacity, row_count), 1)
    selector = (present[:, None, :] == 1) & (ranks[:, None, :] == slot_ids)
    slot_rows = jnp.einsum(
        "ecr,rk->eck", selector.astype(jnp.bfloat16), normed_two, preferred_element_type=jnp.float32
    ).astype(jnp.bfloat16)
    outgoing = jnp.repeat(slot_rows, members, axis=0)
    incoming = lax.all_to_all(outgoing, ("ep", "tp"), split_axis=0, concat_axis=0, tiled=True)
    slot_rows = incoming.reshape(devices * capacity, width)
    expert_hidden = (
        jax.nn.silu(jnp.dot(slot_rows, expert_gate, preferred_element_type=jnp.float32))
        * jnp.dot(slot_rows, expert_up, preferred_element_type=jnp.float32)
    ).astype(jnp.bfloat16)
    expert_result = jnp.dot(expert_hidden, expert_down, preferred_element_type=jnp.float32).reshape(
        devices, capacity, width
    )
    back = lax.all_to_all(
        expert_result.astype(jnp.bfloat16), ("ep", "tp"), split_axis=0, concat_axis=0, tiled=True
    ).astype(expert_result.dtype)
    per_expert = jnp.sum(back.reshape(EXPERTS, members, capacity, width), axis=1)
    expert_term = jnp.einsum("ecr,eck,er->rk", selector.astype(jnp.float32), per_expert, share)
    layer_out = (middle.astype(jnp.float32) + expert_term + dense_term).astype(jnp.bfloat16)
    return (layer_out, new_keys, new_values)


def solution(mesh):
    placed = (
        P("ep", None),
        P(),
        P(None, "tp"),
        P(None, "tp"),
        P(None, "tp"),
        P("tp", None),
        P("tp"),
        P("ep", None, "tp"),
        P("ep", None, "tp"),
        P("ep"),
        P(),
        P(None, ("ep", "tp")),
        P(None, ("ep", "tp")),
        P(("ep", "tp"), None),
        P(None, "ep"),
        P(None, "ep"),
        P("ep", None),
        P(),
        P(("ep", "tp"), None),
        P(("ep", "tp"), None),
    )
    return jax.shard_map(
        shards,
        mesh=mesh,
        in_specs=placed,
        out_specs=(P(("ep", "tp"), None), P("ep", "tp"), P("ep", "tp")),
        check_vma=False,
    )
```

profile of v0, /device:TPU:0, one launch (start us, length us, event | category | flops | bytes accessed | tf_op | source)
XLA Modules:
  0.0 201.0 jit_solution(5162440769318501514)
XLA Ops:
  7.2 0.0 reduce-scatter.3.cloned.1.call-start
  7.2 1.1 fusion.31
  8.3 2.9 %convolution_convert_fusion.4 = bf16[16,1024]{1,0:T(8,128)(2,1)S(1)} fusion(bf16[2048,1024]{1,0:T(8,128)(2,1)} %param.22, bf16[16,2048]{1,0:T(8,128)(2,1)} %param.20, f32[2048]{0:T(1024)} %param.21, f32[16]{0:T(128)S(1)} %add_rsqrt_fusion.1), kind=kOutput, calls=%fused_computation.17 | convolution fusion | flops 67256320 | bytes 4300864 | tf_op jit(solution)/shard_map/dot_general | solution.py:77
  11.3 0.1 reshape.82
  11.4 6.4 %copy.57 = bf16[16,1024,128]{1,2,0:T(8,128)(2,1)} copy(bf16[16,1024,128]{2,1,0:T(8,128)(2,1)} %param.27) | data formatting | bytes 8388608 | tf_op args[7]
  17.8 0.1 add.75
  17.9 0.1 iota_compare_fusion.1
  18.0 2.8 %fusion.4 = f32[16,2,8,1024]{3,2,1,0:T(8,128)S(1)} fusion(bf16[16,2,8,64]{3,2,1,0:T(8,128)(2,1)S(1)} %reshape.82, bf16[16,1024,2,64]{1,3,2,0:T(8,128)(2,1)} %bitcast.71, f32[2,8]{1,0:T(2,128)S(1)} %add.75), kind=kOutput, calls=%fused_computation.13 | convolution fusion | flops 34078720 | bytes 5275712 | tf_op jit(solution)/shard_map/bgrd,bsgd->bgrs/dot_general | solution.py:83
  20.8 1.0 copy-done.1
  21.8 0.7 fusion.18
  22.5 1.7 fusion.19
  24.1 2.8 %copy.74 = f32[16,2,8,8,1]{3,2,1,0,4:T(8,128)S(1)} copy(f32[16,2,8,8,1]{4,3,2,1,0:T(8,128)} %bitcast.73) | data formatting | bytes 16384 | tf_op jit(solution)/shard_map/squeeze | solution.py:30
  26.9 0.2 fusion.34
  27.1 2.6 %add_subtract_fusion = f32[16,2,8,8,128]{4,3,2,1,0:T(8,128)} fusion(f32[16,2,8,8,128]{4,3,2,1,0:T(8,128)} %fusion.19, f32[16,2,8,8,128]{4,2,3,1,0:T(8,128)S(1)} %fusion.18, f32[16,2,8,8]{3,2,1,0:T(8,128)S(1)} %fusion.34), kind=kLoop, calls=%fused_computation.36 | loop fusion | flops 524288 | bytes 3153920 | tf_op jit(solution)/shard_map/sub | solution.py:36
  29.7 2.4 %reshape.85 = f32[16,2,8,1024]{3,2,1,0:T(8,128)} reshape(f32[16,2,8,8,128]{4,3,2,1,0:T(8,128)} %add_subtract_fusion) | data formatting | bytes 2097152 | tf_op jit(solution)/shard_map/reshape | solution.py:36
  32.1 6.5 %copy.62 = bf16[16,1024,128]{1,2,0:T(8,128)(2,1)} copy(bf16[16,1024,128]{2,1,0:T(8,128)(2,1)} %param.28) | data formatting | bytes 8388608 | tf_op args[8]
  38.6 3.8 %convolution_convert_fusion.3 = bf16[16,2,8,64]{3,2,1,0:T(8,128)(2,1)S(1)} fusion(bf16[16,1024,2,64]{1,3,2,0:T(8,128)(2,1)} %bitcast.72, f32[16,2,8,1024]{3,2,1,0:T(8,128)} %reshape.85, f32[16,2,8,1024]{3,2,1,0:T(8,128)S(1)} %copy-done.2, pred[16,1024]{1,0:T(8,128)(4,1)S(1)} %iota_compare_fusion.1), kind=kOutput, calls=%fused_computation.16 | convolution fusion | flops 36454400 | bytes 6340608 | tf_op jit(solution)/shard_map/bgrs,bsgd->bgrd/dot_general | solution.py:94
  42.4 0.1 reshape.87
  42.5 3.5 %convolution_convert_fusion.2 = bf16[16,2048]{1,0:T(8,128)(2,1)} fusion(bf16[16,1024]{1,0:T(8,128)(2,1)S(1)} %reshape.87, bf16[1024,2048]{1,0:T(8,128)(2,1)} %param.25), kind=kOutput, calls=%fused_computation.7 | convolution fusion | flops 67141632 | bytes 4292608 | tf_op jit(solution)/shard_map/dot_general | solution.py:98
  46.0 0.0 reduce-scatter.3.cloned.1.call-update
  46.0 0.1 fusion.6
  46.2 0.1 copy.64
  46.2 0.1 copy.63
  46.4 10.1 %reduce-scatter.3.cloned.1.call-done = bf16[8,2048]{1,0:T(8,128)(2,1)} async-done(((bf16[16,2048]{1,0:T(8,128)(2,1)}), bf16[8,2048]{1,0:T(8,128)(2,1)}) %reduce-scatter.3.cloned.1.call-update) | async-done | bytes 32784 | tf_op jit(solution)/shard_map/reduce_scatter | solution.py:99
  56.4 0.9 fusion.37
  57.3 0.1 fusion.39
  57.4 44.0 %all_gather.3 = bf16[128,2048]{1,0:T(8,128)(2,1)S(1)} all-gather(bf16[8,2048]{1,0:T(8,128)(2,1)S(1)} %fusion.39), channel_id=1, replica_groups=mesh['ep'=16,'tp'=2] {'ep'}, dimensions={0}, use_global_device_ids=true | all-gather | bytes 557056 | tf_op jit(solution)/shard_map/all_gather | solution.py:108
  101.4 0.2 convolution_convert_fusion.1
  101.6 0.1 copy.67
  101.7 1.1 broadcast_in_dim.44
  102.7 2.6 %all-to-all-start = ((bf16[32,3,2048]{2,1,0:T(4,128)(2,1)}), bf16[32,3,2048]{2,1,0:T(4,128)(2,1)S(1)}, u32[]{:S(2)}, u32[]{:S(2)}) async-start(bf16[32,3,2048]{2,1,0:T(4,128)(2,1)} %bitcast.11), calls=%async_computation.1 | async-start | bytes 1048576 | tf_op jit(solution)/shard_map/all_to_all | solution.py:131
  105.3 0.2 reduce-scatter.5.cloned.1.call-start
  105.6 0.2 fusion.10
  105.8 2.2 %fusion.65 = f32[128,448]{0,1:T(8,128)S(1)} fusion(bf16[128,2048]{1,0:T(8,128)(2,1)S(1)} %all_gather.3, bf16[2048,448]{0,1:T(8,128)(2,1)} %param.34), kind=kOutput, calls=%fused_computation.91 | convolution fusion | flops 234881024 | bytes 2588672 | tf_op jit(solution)/shard_map/dot_general | solution.py:111
  108.0 4.0 %convolution_multiply_fusion = f32[128,2048]{1,0:T(8,128)} fusion(bf16[448,2048]{1,0:T(8,128)(2,1)S(1)} %copy-done, bf16[128,2048]{1,0:T(8,128)(2,1)S(1)} %all_gather.3, bf16[2048,448]{0,1:T(8,128)(2,1)} %param.35, f32[128]{0:T(128)S(1)} %fusion.10, f32[128,448]{0,1:T(8,128)S(1)} %fusion.65), kind=kOutput, calls=%fused_computation.2 | convolution fusion | flops 470368256 | bytes 5472768 | tf_op jit(solution)/shard_map/dot_general | solution.py:115
  112.0 8.9 %all-to-all-done = bf16[32,3,2048]{2,1,0:T(4,128)(2,1)S(1)} async-done(((bf16[32,3,2048]{2,1,0:T(4,128)(2,1)}), bf16[32,3,2048]{2,1,0:T(4,128)(2,1)S(1)}, u32[]{:S(2)}, u32[]{:S(2)}) %all-to-all-start) | async-done | bytes 393248 | tf_op jit(solution)/shard_map/all_to_all | solution.py:131
  121.0 0.3 reshape.89
  121.3 4.4 %fusion.64 = f32[96,1792]{1,0:T(8,128)S(1)} fusion(bf16[96,2048]{1,0:T(8,128)(2,1)S(1)} %reshape.89, bf16[2048,1792]{1,0:T(8,128)(2,1)} %param.31), kind=kOutput, calls=%fused_computation.90 | convolution fusion | flops 704643072 | bytes 8421376 | tf_op jit(solution)/shard_map/dot_general | solution.py:134
  125.7 7.8 %convolution_convert_fusion = bf16[96,2048]{1,0:T(8,128)(2,1)S(1)} fusion(bf16[1792,2048]{1,0:T(8,128)(2,1)} %param.33, bf16[96,2048]{1,0:T(8,128)(2,1)S(1)} %reshape.89, bf16[2048,1792]{1,0:T(8,128)(2,1)} %param.32, f32[96,1792]{1,0:T(8,128)S(1)} %fusion.64), kind=kOutput, calls=%fused_computation.5 | convolution fusion | flops 1410514944 | bytes 16154624 | tf_op jit(solution)/shard_map/dot_general | solution.py:137
  133.5 1.0 convert_element_type.98
  134.6 2.9 %all-to-all-start.1 = ((bf16[32,3,2048]{2,1,0:T(4,128)(2,1)}), bf16[32,3,2048]{2,1,0:T(4,128)(2,1)S(1)}, u32[]{:S(2)}, u32[]{:S(2)}) async-start(bf16[32,3,2048]{2,1,0:T(4,128)(2,1)} %convert_element_type.98), calls=%async_computation.2 | async-start | bytes 1048576 | tf_op jit(solution)/shard_map/all_to_all | solution.py:140
  137.5 0.1 copy.65
  137.6 1.9 convolution_convert_fusion.5
  139.5 1.9 convolution_convert_fusion.6
  141.4 13.6 %all-to-all-done.1 = bf16[32,3,2048]{2,1,0:T(4,128)(2,1)S(1)} async-done(((bf16[32,3,2048]{2,1,0:T(4,128)(2,1)}), bf16[32,3,2048]{2,1,0:T(4,128)(2,1)S(1)}, u32[]{:S(2)}, u32[]{:S(2)}) %all-to-all-start.1) | async-done | bytes 393248 | tf_op jit(solution)/shard_map/all_to_all | solution.py:140
  154.9 0.3 convert_reduce_fusion
  155.2 37.3 %reduce-scatter.5.cloned.1.call-done = f32[8,2048]{1,0:T(8,128)} async-done(((f32[128,2048]{1,0:T(8,128)}), f32[8,2048]{1,0:T(8,128)}) %reduce-scatter.5.cloned.1.call-update) | async-done | bytes 65552 | tf_op jit(solution)/shard_map/reduce_scatter | solution.py:117
  192.5 1.7 fusion.3
  (29 shorter events, 0.1 us)
Async XLA Ops:
  7.2 100.8 %copy-start = (bf16[448,2048]{1,0:T(8,128)(2,1)S(1)}, bf16[448,2048]{1,0:T(8,128)(2,1)}, u32[]{:S(2)}) copy-start(bf16[448,2048]{1,0:T(8,128)(2,1)} %param.36) | copy-start | bytes 5505028
  7.2 49.2 %reduce-scatter.3.cloned.1.call-start = ((), (), s32[]{:S(2)}) async-start(), calls=%async_computation.4 | async-start | bytes 98304 | tf_op jit(solution)/shard_map/reduce_scatter | solution.py:99
  11.4 6.4 %copy-start.9 = (f32[16]{0:T(128)S(1)}, f32[16]{0:T(128)}, u32[]{:S(2)}) copy-start(f32[16]{0:T(128)} %param.26) | copy-start | bytes 196
  11.4 6.5 %copy-start.8 = (s32[16]{0:T(128)S(1)}, s32[16]{0:T(128)}, u32[]{:S(2)}) copy-start(s32[16]{0:T(128)} %param.29) | copy-start | bytes 196
  20.8 1.0 copy-start.1
  32.1 6.5 %copy-start.2 = (f32[16,2,8,1024]{3,2,1,0:T(8,128)S(1)}, f32[16,2,8,1024]{3,2,1,0:T(8,128)}, u32[]{:S(2)}) copy-start(f32[16,2,8,1024]{3,2,1,0:T(8,128)} %copy-done.1) | copy-start | bytes 3145732
  38.6 7.4 %copy-start.7 = (s32[8,2]{0,1:T(2,128)S(1)}, s32[8,2]{0,1:T(2,128)}, u32[]{:S(2)}) copy-start(s32[8,2]{0,1:T(2,128)} %param.38) | copy-start | bytes 196
  38.6 7.7 %copy-start.6 = (bf16[2048]{0:T(1024)(128)(2,1)S(1)}, bf16[2048]{0:T(1024)(128)(2,1)}, u32[]{:S(2)}) copy-start(bf16[2048]{0:T(1024)(128)(2,1)} %param.37) | copy-start | bytes 12292
  38.6 17.8 %copy-start.3 = (bf16[16,2048]{1,0:T(8,128)(2,1)S(1)}, bf16[16,2048]{1,0:T(8,128)(2,1)}, u32[]{:S(2)}) copy-start(bf16[16,2048]{1,0:T(8,128)(2,1)} %param.20) | copy-start | bytes 196612
  38.6 18.7 %copy-start.5 = (f32[2048]{0:T(1024)S(1)}, f32[2048]{0:T(1024)}, u32[]{:S(2)}) copy-start(f32[2048]{0:T(1024)} %param.30) | copy-start | bytes 24580
  102.7 18.2 %all-to-all-start = ((bf16[32,3,2048]{2,1,0:T(4,128)(2,1)}), bf16[32,3,2048]{2,1,0:T(4,128)(2,1)S(1)}, u32[]{:S(2)}, u32[]{:S(2)}) async-start(bf16[32,3,2048]{2,1,0:T(4,128)(2,1)} %bitcast.11), calls=%async_computation.1 | async-start | bytes 1048576 | tf_op jit(solution)/shard_map/all_to_all | solution.py:131
  105.3 87.1 %reduce-scatter.5.cloned.1.call-start = ((), (), s32[]{:S(2)}) async-start(), calls=%async_computation.5 | async-start | bytes 1114112 | tf_op jit(solution)/shard_map/reduce_scatter | solution.py:117
  125.7 11.8 %copy-start.10 = (bf16[8,2]{0,1:T(2,128)(2,1)S(1)}, bf16[8,2]{0,1:T(2,128)(2,1)}, u32[]{:S(2)}) copy-start(bf16[8,2]{0,1:T(2,128)(2,1)} %param.39) | copy-start | bytes 100
  125.7 11.9 %copy-start.4 = (f32[2048]{0:T(1024)S(1)}, f32[2048]{0:T(1024)}, u32[]{:S(2)}) copy-start(f32[2048]{0:T(1024)} %param.21) | copy-start | bytes 24580
  134.6 20.3 %all-to-all-start.1 = ((bf16[32,3,2048]{2,1,0:T(4,128)(2,1)}), bf16[32,3,2048]{2,1,0:T(4,128)(2,1)S(1)}, u32[]{:S(2)}, u32[]{:S(2)}) async-start(bf16[32,3,2048]{2,1,0:T(4,128)(2,1)} %convert_element_type.98), calls=%async_computation.2 | async-start | bytes 1048576 | tf_op jit(solution)/shard_map/all_to_all | solution.py:140
Sparse Core Ops, SparseCore 0:
  46.1 10.2 reduce-scatter.2
  112.2 80.2 reduce-scatter.4
where the time goes:
time: 202 us; the launch traced here: 201 us
  waiting for transfers between devices  69.9 us (35%)
  blocking collectives  44 us (22%)
  matrix products  39.3 us (19%)
  local copies, waits for them, and re-layouts  22.1 us (11%)
  between operations  14.3 us (7%)
  starting transfers between devices  5.75 us (3%)
  other arithmetic  5.72 us (3%)
    all_gather x1, blocking collectives, shards(): piece = lax.all_gather(normed_two, 'ep', axis=0, tiled=True)  44 us
    reduce_scatter x1, waiting for transfers between devices, shards(): lax.psum_scatter(dense_terms, 'ep', scatter_dimension=0, tiled=True)  37.3 us
    unnamed x25, local copies, waits for them, and re-layouts  13.9 us
    all_to_all x1, waiting for transfers between devices, shards(): lax.all_to_all(expert_result.astype(jnp.bfloat16), ('ep', 'tp'), split_ax...  13.6 us
    reduce_scatter x1, waiting for transfers between devices, shards(): lax.psum_scatter(partial_value.astype(jnp.bfloat16), 'tp', scatter_dimens...  10.1 us
    all_to_all x1, waiting for transfers between devices, shards(): lax.all_to_all(outgoing, ('ep', 'tp'), split_axis=0, concat_axis=0, tiled...  8.92 us
    dot_general x1, matrix products, shards(): jnp.dot(expert_hidden, expert_down, preferred_element_type=jnp.float32)  7.84 us
    dot_general x1, matrix products, shards(): jnp.dot(slot_rows, expert_gate, preferred_element_type=jnp.float32)  4.37 us
  transfers between devices with their start and end apart: 4, of which 4 were waited for; matrix products, arithmetic and copies ran while one was open for 12% of the time, Pallas kernels for 0%

commit v1 on v0

v1 whole, which is shorter than its diff:
```python
import functools

import jax
import jax.numpy as jnp
from jax import lax
from jax.experimental import pallas as pl
from jax.experimental.pallas import tpu as pltpu
from jax.sharding import PartitionSpec as P

HEAD_DIM = 64
EXPERTS = 8
TOP = 2
EPSILON = 1e-06
LANES = 128
MESH = pl.DeviceIdType.MESH
F32 = jnp.float32
BF16 = jnp.bfloat16


def dot(a, b, dims=((1,), (0,))):
    return lax.dot_general(a, b, (dims, ((), ())), preferred_element_type=F32)


def normed_rows(widened, gain):
    scale = lax.rsqrt(jnp.mean(widened * widened, axis=-1, keepdims=True) + EPSILON)
    return (widened * scale * gain).astype(BF16)


def tile_of(size):
    for tile in (256, 128):
        if size % tile == 0:
            return tile
    return size


def tiled(size, body):
    tile = tile_of(size)
    if tile == size:
        body(pl.ds(0, size))
        return

    def step(i, carry):
        body(pl.ds(pl.multiple_of(i * tile, tile), tile))
        return carry

    lax.fori_loop(0, size // tile, step, 0)


def kernel(
    n_ep, n_tp,
    tokens, norm_attn, bias, lengths, norm_ffn, mix, share,
    wq_hbm, wk_hbm, wv_hbm, wo_hbm, ck_hbm, cv_hbm, eg_hbm, eu_hbm, ed_hbm, dg_hbm, du_hbm, dd_hbm,
    out, new_keys, new_values,
    wq, wk, wv, wo, ck, cv, eg, eu, ed, dg, du, dd,
    q_heads, o_heads, flat, pair_out, pair_in, own_tokens,
    gathered, shares, slots, e_hidden, d_hidden, mine, theirs_out, theirs_in, sums, scatter_out, scatter_in,
    w_sem, k_sem, v_sem, pair_sem, g_send, g_recv, s_send, s_recv, slot_sem, back_sem, r_send, r_recv,
):
    ep, tp = lax.axis_index("ep"), lax.axis_index("tp")
    other = 1 - tp
    seqs, width = tokens.shape
    rows = seqs // n_tp
    cache_len = ck.shape[1]
    heads = bias.shape[0]
    tiles = heads * HEAD_DIM // LANES
    half = heads // 2
    cap = slots.shape[1] // n_ep
    n_rows = n_ep * rows

    barrier = pltpu.get_barrier_semaphore()

    def greet(k, carry):
        peer = lax.rem(ep + k, n_ep)
        pl.semaphore_signal(barrier, inc=1, device_id=(peer, tp), device_id_type=MESH)
        return carry

    pl.semaphore_signal(barrier, inc=1, device_id=(ep, other), device_id_type=MESH)
    lax.fori_loop(1, n_ep, greet, 0)

    pairs = [(wq_hbm, wq), (wk_hbm, wk), (wv_hbm, wv), (wo_hbm, wo), (dg_hbm, dg), (du_hbm, du),
             (eg_hbm, eg), (eu_hbm, eu), (ed_hbm, ed), (dd_hbm, dd)]
    loads = [pltpu.make_async_copy(a, b, w_sem.at[i]) for i, (a, b) in enumerate(pairs)]
    l_wq, l_wk, l_wv, l_wo, l_dg, l_du, l_eg, l_eu, l_ed, l_dd = loads

    def key_load(b):
        return pltpu.make_async_copy(ck_hbm.at[b], ck.at[b], k_sem.at[b])

    def value_load(b):
        return pltpu.make_async_copy(cv_hbm.at[b], cv.at[b], v_sem.at[b])

    l_wq.start()
    l_wk.start()
    l_wv.start()

    def start_cache(b, carry):
        key_load(b).start()
        value_load(b).start()
        return carry

    lax.fori_loop(0, seqs, start_cache, 0)
    for load in (l_wo, l_dg, l_du, l_eg, l_eu, l_ed, l_dd):
        load.start()

    widened = tokens[...].astype(F32)
    own_tokens[...] = widened.reshape(n_tp, rows, width)
    normed = normed_rows(widened, norm_attn[...])
    l_wq.wait()
    lane = lax.broadcasted_iota(jnp.int32, (seqs, LANES), 1)
    low = lane < HEAD_DIM
    for j in range(tiles):
        tile = dot(normed, wq[:, j * LANES:(j + 1) * LANES]).astype(BF16).astype(F32)
        rolled = pltpu.roll(tile, HEAD_DIM, 1)
        for side in range(2):
            head = 2 * j + side
            group = head // half
            value = tile if side == group else rolled
            q_heads[:, head, :] = jnp.where(low if group == 0 else ~low, value, 0.0)
    l_wk.wait()
    new_keys[...] = dot(normed, wk[...]).astype(BF16)
    l_wv.wait()
    new_values[...] = dot(normed, wv[...]).astype(BF16)

    blocks = cache_len // LANES
    tri = (
        lax.broadcasted_iota(jnp.int32, (LANES, LANES), 0)
        > lax.broadcasted_iota(jnp.int32, (LANES, LANES), 1)
    ).astype(F32).astype(BF16)
    places = lax.broadcasted_iota(jnp.int32, (heads, cache_len), 1)
    offsets = bias[...]

    def attend(b):
        key_load(b).wait()
        query = q_heads[b].astype(BF16)
        z = dot(query, ck[b], ((1,), (1,))) * HEAD_DIM ** (-0.5) + offsets
        visible = places < lengths[b]
        soft = jnp.log(1.0 + jnp.exp(-jnp.abs(z)))
        take = jnp.minimum(z, 0.0) - soft
        keep = jnp.where(visible, jnp.minimum(-z, 0.0) - soft, 0.0)
        stack = jnp.concatenate([keep[:, n * LANES:(n + 1) * LANES] for n in range(blocks)], axis=0)
        high = stack.astype(BF16)
        rest = (stack - high.astype(F32)).astype(BF16)
        within = dot(high, tri) + dot(rest, tri)
        totals = jnp.sum(stack, axis=1, keepdims=True)
        carry = jnp.zeros((heads, 1), F32)
        after = [None] * blocks
        for n in range(blocks - 1, -1, -1):
            after[n] = within[n * heads:(n + 1) * heads] + carry
            carry = carry + totals[n * heads:(n + 1) * heads]
        weight = jnp.where(visible, jnp.exp(take + jnp.concatenate(after, axis=1)), 0.0).astype(BF16)
        value_load(b).wait()
        o_heads[b] = dot(weight, cv[b]).astype(BF16).astype(F32)

    step_seqs = 2 if seqs % 2 == 0 else 1

    def attend_step(t, carry):
        for i in range(step_seqs):
            attend(t * step_seqs + i)
        return carry

    lax.fori_loop(0, seqs // step_seqs, attend_step, 0)

    for j in range(tiles):
        first, second = o_heads[:, 2 * j, :], o_heads[:, 2 * j + 1, :]
        if 2 * j < half:
            second = pltpu.roll(second, HEAD_DIM, 1)
        else:
            first = pltpu.roll(first, HEAD_DIM, 1)
        flat[:, j * LANES:(j + 1) * LANES] = jnp.where(low, first, second).astype(BF16)
    l_wo.wait()

    def project(cols):
        value = dot(flat[...], wo[:, cols]).astype(BF16).astype(F32)
        pair_out[:, :, cols] = value.reshape(n_tp, rows, value.shape[1])

    tiled(width, project)

    pl.semaphore_wait(barrier, n_ep)
    pair_copy = pltpu.make_async_remote_copy(
        pair_out.at[other], pair_in, pair_sem.at[0], pair_sem.at[1],
        device_id=(ep, other), device_id_type=MESH)
    pair_copy.start()
    shares[ep] = share[...]
    pair_copy.wait_recv()
    middle = (own_tokens[tp] + (pair_out[tp] + pair_in[...])).astype(BF16).astype(F32)
    gathered[ep] = normed_rows(middle, norm_ffn[...])

    def gather_copy(dest, block, index):
        return pltpu.make_async_remote_copy(
            gathered.at[block], gathered.at[block], g_send.at[index], g_recv.at[block],
            device_id=(dest, tp), device_id_type=MESH)

    def share_copy(dest, block, index):
        return pltpu.make_async_remote_copy(
            share, shares.at[block], s_send.at[index], s_recv.at[block],
            device_id=(dest, tp), device_id_type=MESH)

    def send_rows(k, carry):
        dest = lax.rem(ep + k, n_ep)
        share_copy(dest, ep, dest).start()
        gather_copy(dest, ep, dest).start()
        return carry

    def await_rows(k, carry):
        source = lax.rem(ep + k, n_ep)
        share_copy(source, source, source).wait_recv()
        gather_copy(source, source, source).wait_recv()
        return carry

    lax.fori_loop(1, n_ep, send_rows, 0)
    lax.fori_loop(1, n_ep, await_rows, 0)

    everything = gathered[...].astype(F32).reshape(n_rows, width)
    mix_gate = jax.nn.sigmoid(jnp.sum(everything * mix[...], axis=1, keepdims=True))
    everything = everything.astype(BF16)

    members = n_ep * n_tp // EXPERTS
    expert = (ep * n_tp + tp) // members
    share_all = shares[...].reshape(n_rows, LANES).astype(BF16)
    one_hot = (lax.broadcasted_iota(jnp.int32, (8, LANES), 1) == expert).astype(F32).astype(BF16)
    share_row = dot(one_hot, share_all, ((1,), (1,)))
    present = (share_row > 0.0).astype(F32)
    row_j = lax.broadcasted_iota(jnp.int32, (n_rows, n_rows), 0)
    row_i = lax.broadcasted_iota(jnp.int32, (n_rows, n_rows), 1)
    shift = rows.bit_length() - 1
    same = ((row_j >> shift) == (row_i >> shift)) & (row_j <= row_i)
    rank = dot(present.astype(BF16), same.astype(F32).astype(BF16)) - 1.0
    n_slots = n_ep * cap
    slot = lax.broadcasted_iota(jnp.int32, (n_slots, n_rows), 0)
    block = lax.broadcasted_iota(jnp.int32, (n_slots, n_rows), 1) >> shift
    picked = ((slot - cap * block).astype(F32) == rank[0:1]) & (present[0:1] > 0.0)
    selector = picked.astype(F32)
    slot_share = jnp.sum(selector * share_row[0:1], axis=1, keepdims=True)
    selector = selector.astype(BF16)
    slots[0] = dot(selector, everything).astype(BF16)
    slot_copy = pltpu.make_async_remote_copy(
        slots.at[0], slots.at[1], slot_sem.at[0], slot_sem.at[1],
        device_id=(ep, other), device_id_type=MESH)
    slot_copy.start()

    l_dg.wait()
    l_du.wait()

    def dense_up(cols):
        up = dot(everything, du[:, cols])
        d_hidden[:, cols] = (jax.nn.silu(dot(everything, dg[:, cols])) * up).astype(BF16)

    tiled(d_hidden.shape[1], dense_up)

    l_eg.wait()
    l_eu.wait()
    slot_copy.wait_recv()
    slot_rows = slots[...].reshape(2 * n_slots, width)

    def expert_up(cols):
        up = dot(slot_rows, eu[:, cols])
        e_hidden[:, cols] = (jax.nn.silu(dot(slot_rows, eg[:, cols])) * up).astype(BF16)

    tiled(e_hidden.shape[1], expert_up)
    l_ed.wait()

    def expert_down(cols):
        value = dot(e_hidden[...], ed[:, cols])
        mine[:, cols] = value[:n_slots]
        theirs_out[:, cols] = value[n_slots:].astype(BF16)

    tiled(width, expert_down)
    back_copy = pltpu.make_async_remote_copy(
        theirs_out, theirs_in, back_sem.at[0], back_sem.at[1],
        device_id=(ep, other), device_id_type=MESH)
    back_copy.start()
    l_dd.wait()

    def dense_down(cols):
        sums[:, cols] = dot(d_hidden[...], dd[:, cols]) * mix_gate

    tiled(width, dense_down)
    back_copy.wait_recv()

    def combine(cols):
        result = ((mine[:, cols] + theirs_in[:, cols].astype(F32)) * slot_share).astype(BF16)
        total = sums[:, cols] + dot(selector, result, ((0,), (0,)))
        scatter_out[:, :, cols] = total.reshape(n_ep, rows, total.shape[1]).astype(BF16)

    tiled(width, combine)

    def scatter_copy(dest, source):
        return pltpu.make_async_remote_copy(
            scatter_out.at[dest], scatter_in.at[source], r_send.at[dest], r_recv.at[source],
            device_id=(dest, tp), device_id_type=MESH)

    def send_sums(k, carry):
        dest = lax.rem(ep + k, n_ep)
        scatter_copy(dest, ep).start()
        return carry

    lax.fori_loop(1, n_ep, send_sums, 0)

    def add_sums(k, total):
        source = lax.rem(ep + n_ep - k, n_ep)
        scatter_copy(source, source).wait_recv()
        return total + scatter_in[source].astype(F32)

    total = lax.fori_loop(1, n_ep, add_sums, middle + scatter_out[ep].astype(F32))
    out[...] = total.astype(BF16)

    pair_copy.wait_send()
    slot_copy.wait_send()
    back_copy.wait_send()

    def finish(k, carry):
        dest = lax.rem(ep + k, n_ep)
        share_copy(dest, ep, dest).wait_send()
        gather_copy(dest, ep, dest).wait_send()
        scatter_copy(dest, ep).wait_send()
        return carry

    lax.fori_loop(1, n_ep, finish, 0)


def shards(
    n_ep, n_tp,
    tokens, norm_attn, w_query, w_key, w_value, w_out, attn_bias, cache_keys, cache_values, lengths,
    norm_ffn, expert_gate, expert_up, expert_down, dense_gate_w, dense_up_w, dense_down_w, dense_mix,
    routes, route_weights,
):
    seqs, width = tokens.shape
    rows = seqs // n_tp
    heads = attn_bias.shape[0]
    cap = (rows * TOP + EXPERTS - 1) // EXPERTS + 1
    ids = lax.broadcasted_iota(jnp.int32, (1, 1, LANES), 2)
    matched = routes[:, :, None] == ids
    share = jnp.sum(jnp.where(matched, route_weights.astype(F32)[:, :, None], 0.0), axis=1)
    weights = (w_query, w_key, w_value, w_out, cache_keys, cache_values, expert_gate, expert_up,
               expert_down, dense_gate_w, dense_up_w, dense_down_w)
    vmem = pl.BlockSpec(memory_space=pltpu.VMEM)
    smem = pl.BlockSpec(memory_space=pltpu.SMEM)
    hbm = pl.BlockSpec(memory_space=pl.ANY)
    n_slots = n_ep * cap
    ff, dense_ff = expert_gate.shape[1], dense_gate_w.shape[1]
    dma = pltpu.SemaphoreType.DMA
    scratch = [pltpu.VMEM(w.shape, w.dtype) for w in weights] + [
        pltpu.VMEM((seqs, heads, LANES), F32),
        pltpu.VMEM((seqs, heads, LANES), F32),
        pltpu.VMEM((seqs, heads * HEAD_DIM), BF16),
        pltpu.VMEM((n_tp, rows, width), F32),
        pltpu.VMEM((rows, width), F32),
        pltpu.VMEM((n_tp, rows, width), F32),
        pltpu.VMEM((n_ep, rows, width), BF16),
        pltpu.VMEM((n_ep, rows, LANES), F32),
        pltpu.VMEM((2, n_slots, width), BF16),
        pltpu.VMEM((2 * n_slots, ff), BF16),
        pltpu.VMEM((n_ep * rows, dense_ff), BF16),
        pltpu.VMEM((n_slots, width), F32),
        pltpu.VMEM((n_slots, width), BF16),
        pltpu.VMEM((n_slots, width), BF16),
        pltpu.VMEM((n_ep * rows, width), F32),
        pltpu.VMEM((n_ep, rows, width), BF16),
        pltpu.VMEM((n_ep, rows, width), BF16),
        dma((10,)), dma((seqs,)), dma((seqs,)), dma((2,)),
        dma((n_ep,)), dma((n_ep,)), dma((n_ep,)), dma((n_ep,)),
        dma((2,)), dma((2,)), dma((n_ep,)), dma((n_ep,)),
    ]
    return pl.pallas_call(
        functools.partial(kernel, n_ep, n_tp),
        out_shape=(
            jax.ShapeDtypeStruct((rows, width), BF16),
            jax.ShapeDtypeStruct((seqs, w_key.shape[1]), BF16),
            jax.ShapeDtypeStruct((seqs, w_value.shape[1]), BF16),
        ),
        in_specs=[vmem, vmem, vmem, smem, vmem, vmem, vmem] + [hbm] * 12,
        out_specs=(vmem, vmem, vmem),
        scratch_shapes=scratch,
        compiler_params=pltpu.CompilerParams(
            collective_id=0, has_side_effects=True, vmem_limit_bytes=67043328
        ),
    )(tokens, norm_attn[None], attn_bias[:, None], lengths, norm_ffn[None],
      dense_mix.astype(F32)[None], share, *weights)


def solution(mesh):
    placed = (
        P("ep", None),
        P(),
        P(None, "tp"),
        P(None, "tp"),
        P(None, "tp"),
        P("tp", None),
        P("tp"),
        P("ep", None, "tp"),
        P("ep", None, "tp"),
        P("ep"),
        P(),
        P(None, ("ep", "tp")),
        P(None, ("ep", "tp")),
        P(("ep", "tp"), None),
        P(None, "ep"),
        P(None, "ep"),
        P("ep", None),
        P(),
        P(("ep", "tp"), None),
        P(("ep", "tp"), None),
    )
    return jax.shard_map(
        functools.partial(shards, mesh.shape["ep"], mesh.shape["tp"]),
        mesh=mesh,
        in_specs=placed,
        out_specs=(P(("ep", "tp"), None), P("ep", "tp"), P("ep", "tp")),
        check_vma=False,
    )
```

time: 202 us -> 74.6 us (0.37)
  the two profiles are of different devices: /device:TPU:0 before, /device:TPU:28 now
where the time goes in v1:
time: 74.6 us; the launch traced here: 74.2 us
  Pallas kernels  58.6 us (79%)
  local copies, waits for them, and re-layouts  11.5 us (15%)
  other arithmetic  3.42 us (5%)
    pallas_call x1, Pallas kernels, shards(): pl.pallas_call(functools.partial(kernel, n_ep, n_tp), out_shape=(jax.Shap...  58.6 us
    unnamed x7, local copies, waits for them, and re-layouts  10.2 us

profile of v1, /device:TPU:28, one launch (start us, length us, event | category | flops | bytes accessed | tf_op | source)
XLA Modules:
  0.0 74.2 jit_solution(839317861568595988)
XLA Ops:
  0.6 0.0 copy-start
  0.6 0.8 %convert_element_type.4 = f32[8,2]{0,1:T(2,128)S(1)} convert(bf16[8,2]{0,1:T(2,128)(2,1)} %param.39) | non-fusion elementwise | flops 16 | bytes 96 | tf_op jit(solution)/shard_map/convert_element_type | solution.py:332
  1.4 1.3 %select_reduce_fusion.share = f32[8,128]{1,0:T(8,128)} fusion(f32[8,2]{0,1:T(2,128)S(1)} %convert_element_type.4, s32[8,2]{0,1:T(2,128)} %param.38), kind=kLoop, calls=%fused_computation | loop fusion | flops 5120 | bytes 4224 | tf_op jit(solution)/shard_map/reduce_sum | solution.py:332
  2.8 1.3 %copy.28.bias = f32[16,1]{1,0:T(8,128)} copy(f32[16,1]{0,1:T(1,128)} %bitcast.7) | data formatting | bytes 128 | tf_op jit(solution)/shard_map/broadcast_in_dim | solution.py:376
  4.1 1.3 %broadcast_in_dim.35 = f32[2048]{0:T(1024)} convert(bf16[2048]{0:T(1024)(128)(2,1)} %param.37) | non-fusion elementwise | flops 2048 | bytes 12288 | tf_op jit(solution)/shard_map/broadcast_in_dim | solution.py:377
  5.4 3.8 %copy.29.dg_hbm = bf16[2048,448]{1,0:T(8,128)(2,1)} copy(bf16[2048,448]{0,1:T(8,128)(2,1)} %param.34) | data formatting | bytes 3670016 | tf_op args[14]
  9.2 0.0 copy-done
  9.2 2.5 %copy.30.du_hbm = bf16[2048,448]{1,0:T(8,128)(2,1)} copy(bf16[2048,448]{0,1:T(8,128)(2,1)S(1)} %copy-done) | data formatting | bytes 3670016 | tf_op args[15]
  11.7 58.6 %shard_map.211 = (bf16[8,2048]{1,0:T(8,128)(2,1)}, bf16[16,128]{1,0:T(8,128)(2,1)}, bf16[16,128]{1,0:T(8,128)(2,1)}) custom-call(bf16[16,2048]{1,0:T(8,128)(2,1)} %tokens.1, f32[1,2048]{1,0:T(1,128)} %bitcast.5, f32[16,1]{1,0:T(8,128)} %copy.28.bias, s32[16]{0:T(128)} %lengths.1, f32[1,2048]{1,0:T(1,128)} %bitcast.6, f32[1,2048]{1,0:T(1,128)} %bitcast.4, ...), custom_call_target="tpu_custom_call" | custom-call | tf_op jit(solution)/shard_map/pallas_call | solution.py:363
  70.3 1.4 %copy.34 = bf16[8,2048]{1,0:T(8,128)(2,1)} copy(bf16[8,2048]{1,0:T(8,128)(2,1)} %get-tuple-element.6) | data formatting | bytes 65536
  71.6 1.3 %copy.35 = bf16[16,128]{1,0:T(8,128)(2,1)} copy(bf16[16,128]{1,0:T(8,128)(2,1)} %get-tuple-element.7) | data formatting | bytes 8192
  72.9 1.3 %copy.36 = bf16[16,128]{1,0:T(8,128)(2,1)} copy(bf16[16,128]{1,0:T(8,128)(2,1)} %get-tuple-element.8) | data formatting | bytes 8192
Async XLA Ops:
  0.6 8.6 %copy-start = (bf16[2048,448]{0,1:T(8,128)(2,1)S(1)}, bf16[2048,448]{0,1:T(8,128)(2,1)}, u32[]{:S(2)}) copy-start(bf16[2048,448]{0,1:T(8,128)(2,1)} %param.35) | copy-start | bytes 5505028

commit v2 on v1

--- a/solution.py
+++ b/solution.py
@@ -33,14 +33,14 @@
     return size
 
 
-def tiled(size, body):
+def tiled(size, body, start=0):
     tile = tile_of(size)
     if tile == size:
-        body(pl.ds(0, size))
+        body(pl.ds(start, size))
         return
 
     def step(i, carry):
-        body(pl.ds(pl.multiple_of(i * tile, tile), tile))
+        body(pl.ds(pl.multiple_of(i * tile + start, tile), tile))
         return carry
 
     lax.fori_loop(0, size // tile, step, 0)
@@ -48,12 +48,12 @@
 
 def kernel(
     n_ep, n_tp,
-    tokens, norm_attn, bias, lengths, norm_ffn, mix, share,
+    tokens, norm_attn, bias, lengths, norm_ffn, mix, routes, route_weights,
     wq_hbm, wk_hbm, wv_hbm, wo_hbm, ck_hbm, cv_hbm, eg_hbm, eu_hbm, ed_hbm, dg_hbm, du_hbm, dd_hbm,
     out, new_keys, new_values,
     wq, wk, wv, wo, ck, cv, eg, eu, ed, dg, du, dd,
-    q_heads, o_heads, flat, pair_out, pair_in, own_tokens,
-    gathered, shares, slots, e_hidden, d_hidden, mine, theirs_out, theirs_in, sums, scatter_out, scatter_in,
+    q_heads, o_heads, flat, pair_out, pair_in, own_tokens, share,
+    gathered, shares, slots, e_hidden, d_hidden, mine, theirs_out, theirs_in, scatter_out, scatter_in,
     w_sem, k_sem, v_sem, pair_sem, g_send, g_recv, s_send, s_recv, slot_sem, back_sem, r_send, r_recv,
 ):
     ep, tp = lax.axis_index("ep"), lax.axis_index("tp")
@@ -100,6 +100,17 @@
     lax.fori_loop(0, seqs, start_cache, 0)
     for load in (l_wo, l_dg, l_du, l_eg, l_eu, l_ed, l_dd):
         load.start()
+
+    ids = lax.broadcasted_iota(jnp.int32, (LANES, rows), 0)
+    share_columns = jnp.zeros((LANES, rows), F32)
+    for choice in range(TOP):
+        chosen = ids == routes[choice:choice + 1, :]
+        value = route_weights[choice:choice + 1, :].astype(F32)
+        share_columns = share_columns + jnp.where(chosen, value, 0.0)
+    diagonal = (
+        lax.broadcasted_iota(jnp.int32, (rows, rows), 0) == lax.broadcasted_iota(jnp.int32, (rows, rows), 1)
+    ).astype(F32).astype(BF16)
+    share[...] = dot(diagonal, share_columns.astype(BF16), ((1,), (1,)))
 
     widened = tokens[...].astype(F32)
     own_tokens[...] = widened.reshape(n_tp, rows, width)
@@ -126,10 +137,13 @@
         > lax.broadcasted_iota(jnp.int32, (LANES, LANES), 1)
     ).astype(F32).astype(BF16)
     places = lax.broadcasted_iota(jnp.int32, (heads, cache_len), 1)
-    offsets = bias[...]
+    head_ids = lax.broadcasted_iota(jnp.int32, (heads, LANES), 0)
+    offsets = jnp.zeros((heads, LANES), F32)
+    for head in range(heads):
+        offsets = jnp.where(head_ids == head, bias[head], offsets)
+    offsets = jnp.concatenate([offsets] * blocks, axis=1)
 
     def attend(b):
-        key_load(b).wait()
         query = q_heads[b].astype(BF16)
         z = dot(query, ck[b], ((1,), (1,))) * HEAD_DIM ** (-0.5) + offsets
         visible = places < lengths[b]
@@ -147,14 +161,17 @@
             after[n] = within[n * heads:(n + 1) * heads] + carry
             carry = carry + totals[n * heads:(n + 1) * heads]
         weight = jnp.where(visible, jnp.exp(take + jnp.concatenate(after, axis=1)), 0.0).astype(BF16)
-        value_load(b).wait()
-        o_heads[b] = dot(weight, cv[b]).astype(BF16).astype(F32)
-
-    step_seqs = 2 if seqs % 2 == 0 else 1
+        return dot(weight, cv[b]).astype(BF16).astype(F32)
+
+    step_seqs = 4 if seqs % 4 == 0 else 1
 
     def attend_step(t, carry):
         for i in range(step_seqs):
-            attend(t * step_seqs + i)
+            key_load(t * step_seqs + i).wait()
+            value_load(t * step_seqs + i).wait()
+        mixed = [attend(t * step_seqs + i) for i in range(step_seqs)]
+        for i in range(step_seqs):
+            o_heads[t * step_seqs + i] = mixed[i]
         return carry
 
     lax.fori_loop(0, seqs // step_seqs, attend_step, 0)
@@ -210,7 +227,7 @@
     lax.fori_loop(1, n_ep, await_rows, 0)
 
     everything = gathered[...].astype(F32).reshape(n_rows, width)
-    mix_gate = jax.nn.sigmoid(jnp.sum(everything * mix[...], axis=1, keepdims=True))
+    mix_gate = jax.nn.sigmoid(jnp.sum(everything * mix[...].astype(F32), axis=1, keepdims=True))
     everything = everything.astype(BF16)
 
     members = n_ep * n_tp // EXPERTS
@@ -240,11 +257,9 @@
     l_dg.wait()
     l_du.wait()
 
-    def dense_up(cols):
-        up = dot(everything, du[:, cols])
-        d_hidden[:, cols] = (jax.nn.silu(dot(everything, dg[:, cols])) * up).astype(BF16)
-
-    tiled(d_hidden.shape[1], dense_up)
+    across = ((1,), (1,))
+    up = dot(everything, du[...], across)
+    d_hidden[...] = (jax.nn.silu(dot(everything, dg[...], across)) * up).astype(BF16)
 
     l_eg.wait()
     l_eu.wait()
@@ -258,60 +273,62 @@
     tiled(e_hidden.shape[1], expert_up)
     l_ed.wait()
 
-    def expert_down(cols):
-        value = dot(e_hidden[...], ed[:, cols])
-        mine[:, cols] = value[:n_slots]
-        theirs_out[:, cols] = value[n_slots:].astype(BF16)
-
-    tiled(width, expert_down)
-    back_copy = pltpu.make_async_remote_copy(
-        theirs_out, theirs_in, back_sem.at[0], back_sem.at[1],
-        device_id=(ep, other), device_id_type=MESH)
-    back_copy.start()
+    chunks = scatter_out.shape[0]
+    part = width // chunks
+
+    def back_copy(c):
+        return pltpu.make_async_remote_copy(
+            theirs_out.at[c], theirs_in.at[c], back_sem.at[0, c], back_sem.at[1, c],
+            device_id=(ep, other), device_id_type=MESH)
+
+    def scatter_copy(c, dest, source):
+        return pltpu.make_async_remote_copy(
+            scatter_out.at[c, dest], scatter_in.at[c, source], r_send.at[c, dest], r_recv.at[c, source],
+            device_id=(dest, tp), device_id_type=MESH)
+
+    for c in range(chunks):
+        value = dot(e_hidden[...], ed[:, c * part:(c + 1) * part])
+        mine[c] = value[:n_slots]
+        theirs_out[c] = value[n_slots:].astype(BF16)
+        back_copy(c).start()
     l_dd.wait()
 
-    def dense_down(cols):
-        sums[:, cols] = dot(d_hidden[...], dd[:, cols]) * mix_gate
-
-    tiled(width, dense_down)
-    back_copy.wait_recv()
-
-    def combine(cols):
-        result = ((mine[:, cols] + theirs_in[:, cols].astype(F32)) * slot_share).astype(BF16)
-        total = sums[:, cols] + dot(selector, result, ((0,), (0,)))
-        scatter_out[:, :, cols] = total.reshape(n_ep, rows, total.shape[1]).astype(BF16)
-
-    tiled(width, combine)
-
-    def scatter_copy(dest, source):
-        return pltpu.make_async_remote_copy(
-            scatter_out.at[dest], scatter_in.at[source], r_send.at[dest], r_recv.at[source],
-            device_id=(dest, tp), device_id_type=MESH)
-
-    def send_sums(k, carry):
-        dest = lax.rem(ep + k, n_ep)
-        scatter_copy(dest, ep).start()
-        return carry
-
-    lax.fori_loop(1, n_ep, send_sums, 0)
-
-    def add_sums(k, total):
-        source = lax.rem(ep + n_ep - k, n_ep)
-        scatter_copy(source, source).wait_recv()
-        return total + scatter_in[source].astype(F32)
-
-    total = lax.fori_loop(1, n_ep, add_sums, middle + scatter_out[ep].astype(F32))
-    out[...] = total.astype(BF16)
+    for c in range(chunks):
+        total = dot(d_hidden[...], dd[:, c * part:(c + 1) * part]) * mix_gate
+        back_copy(c).wait_recv()
+        result = ((mine[c] + theirs_in[c].astype(F32)) * slot_share).astype(BF16)
+        total = total + dot(selector, result, ((0,), (0,)))
+        scatter_out[c] = total.reshape(n_ep, rows, part).astype(BF16)
+
+        def send_sums(k, carry):
+            dest = lax.rem(ep + k, n_ep)
+            scatter_copy(c, dest, ep).start()
+            return carry
+
+        lax.fori_loop(1, n_ep, send_sums, 0)
+
+    for c in range(chunks):
+
+        def add_sums(k, total):
+            source = lax.rem(ep + n_ep - k, n_ep)
+            scatter_copy(c, source, source).wait_recv()
+            return total + scatter_in[c, source].astype(F32)
+
+        begin = middle[:, c * part:(c + 1) * part] + scatter_out[c, ep].astype(F32)
+        total = lax.fori_loop(1, n_ep, add_sums, begin)
+        out[:, c * part:(c + 1) * part] = total.astype(BF16)
 
     pair_copy.wait_send()
     slot_copy.wait_send()
-    back_copy.wait_send()
+    for c in range(chunks):
+        back_copy(c).wait_send()
 
     def finish(k, carry):
         dest = lax.rem(ep + k, n_ep)
         share_copy(dest, ep, dest).wait_send()
         gather_copy(dest, ep, dest).wait_send()
-        scatter_copy(dest, ep).wait_send()
+        for c in range(chunks):
+            scatter_copy(c, dest, ep).wait_send()
         return carry
 
     lax.fori_loop(1, n_ep, finish, 0)
@@ -327,11 +344,10 @@
     rows = seqs // n_tp
     heads = attn_bias.shape[0]
     cap = (rows * TOP + EXPERTS - 1) // EXPERTS + 1
-    ids = lax.broadcasted_iota(jnp.int32, (1, 1, LANES), 2)
-    matched = routes[:, :, None] == ids
-    share = jnp.sum(jnp.where(matched, route_weights.astype(F32)[:, :, None], 0.0), axis=1)
+    chunks = 4 if width % 512 == 0 else 1
+    part = width // chunks
     weights = (w_query, w_key, w_value, w_out, cache_keys, cache_values, expert_gate, expert_up,
-               expert_down, dense_gate_w, dense_up_w, dense_down_w)
+               expert_down, dense_gate_w.T, dense_up_w.T, dense_down_w)
     vmem = pl.BlockSpec(memory_space=pltpu.VMEM)
     smem = pl.BlockSpec(memory_space=pltpu.SMEM)
     hbm = pl.BlockSpec(memory_space=pl.ANY)
@@ -345,36 +361,48 @@
         pltpu.VMEM((n_tp, rows, width), F32),
         pltpu.VMEM((rows, width), F32),
         pltpu.VMEM((n_tp, rows, width), F32),
+        pltpu.VMEM((rows, LANES), F32),
         pltpu.VMEM((n_ep, rows, width), BF16),
         pltpu.VMEM((n_ep, rows, LANES), F32),
         pltpu.VMEM((2, n_slots, width), BF16),
         pltpu.VMEM((2 * n_slots, ff), BF16),
         pltpu.VMEM((n_ep * rows, dense_ff), BF16),
-        pltpu.VMEM((n_slots, width), F32),
-        pltpu.VMEM((n_slots, width), BF16),
-        pltpu.VMEM((n_slots, width), BF16),
-        pltpu.VMEM((n_ep * rows, width), F32),
-        pltpu.VMEM((n_ep, rows, width), BF16),
-        pltpu.VMEM((n_ep, rows, width), BF16),
+        pltpu.VMEM((chunks, n_slots, part), F32),
+        pltpu.VMEM((chunks, n_slots, part), BF16),
+        pltpu.VMEM((chunks, n_slots, part), BF16),
+        pltpu.VMEM((chunks, n_ep, rows, part), BF16),
+        pltpu.VMEM((chunks, n_ep, rows, part), BF16),
         dma((10,)), dma((seqs,)), dma((seqs,)), dma((2,)),
         dma((n_ep,)), dma((n_ep,)), dma((n_ep,)), dma((n_ep,)),
-        dma((2,)), dma((2,)), dma((n_ep,)), dma((n_ep,)),
+        dma((2,)), dma((2, chunks)), dma((chunks, n_ep)), dma((chunks, n_ep)),
     ]
-    return pl.pallas_call(
+    results = pl.pallas_call(
         functools.partial(kernel, n_ep, n_tp),
         out_shape=(
             jax.ShapeDtypeStruct((rows, width), BF16),
             jax.ShapeDtypeStruct((seqs, w_key.shape[1]), BF16),
             jax.ShapeDtypeStruct((seqs, w_value.shape[1]), BF16),
         ),
-        in_specs=[vmem, vmem, vmem, smem, vmem, vmem, vmem] + [hbm] * 12,
+        in_specs=[vmem, vmem, smem, smem, vmem, vmem, vmem, vmem] + [hbm] * 12,
         out_specs=(vmem, vmem, vmem),
         scratch_shapes=scratch,
         compiler_params=pltpu.CompilerParams(
             collective_id=0, has_side_effects=True, vmem_limit_bytes=67043328
         ),
-    )(tokens, norm_attn[None], attn_bias[:, None], lengths, norm_ffn[None],
-      dense_mix.astype(F32)[None], share, *weights)
+    )(tokens, norm_attn[None], attn_bias, lengths, norm_ffn[None],
+      dense_mix[None], routes.T, route_weights.T, *weights)
+    return pl.pallas_call(
+        hand_over,
+        out_shape=tuple(jax.ShapeDtypeStruct(r.shape, r.dtype) for r in results),
+        in_specs=[vmem] * 3,
+        out_specs=(vmem, vmem, vmem),
+    )(*results)
+
+
+def hand_over(a, b, c, a_out, b_out, c_out):
+    a_out[...] = a[...]
+    b_out[...] = b[...]
+    c_out[...] = c[...]
 
 
 def solution(mesh):

time: 74.6 us -> 58.4 us (0.78)
  the two profiles are of different devices: /device:TPU:28 before, /device:TPU:0 now
where the time goes in v2:
time: 58.4 us; the launch traced here: 58.1 us
  Pallas kernels  56.2 us (96%)
  local copies, waits for them, and re-layouts  1.29 us (2%)
  between operations  0.64 us (1%)
    pallas_call x1, Pallas kernels, shards(): pl.pallas_call(functools.partial(kernel, n_ep, n_tp), out_shape=(jax.Shap...  54.8 us
    pallas_call x1, Pallas kernels, shards(): pl.pallas_call(hand_over, out_shape=tuple((jax.ShapeDtypeStruct(r.shape,...  1.39 us
    broadcast_in_dim x1, local copies, waits for them, and re-layouts, shards(): dense_mix[None]  1.29 us

profile of v2, /device:TPU:0, one launch (start us, length us, event | category | flops | bytes accessed | tf_op | source)
XLA Modules:
  0.0 58.1 jit_solution(9557628927888658038)
XLA Ops:
  0.6 1.3 %broadcast_in_dim.11.mix = bf16[1,2048]{1,0:T(2,128)(2,1)} reshape(bf16[2048]{0:T(1024)(128)(2,1)} %param.37) | data formatting | bytes 8192 | tf_op jit(solution)/shard_map/broadcast_in_dim | solution.py:393
  1.9 54.8 %shard_map.211 = (bf16[8,2048]{1,0:T(8,128)(2,1)}, bf16[16,128]{1,0:T(8,128)(2,1)}, bf16[16,128]{1,0:T(8,128)(2,1)}) custom-call(bf16[16,2048]{1,0:T(8,128)(2,1)} %tokens.1, f32[1,2048]{1,0:T(1,128)} %bitcast.8, f32[16]{0:T(128)} %bias.1, s32[16]{0:T(128)} %lengths.1, f32[1,2048]{1,0:T(1,128)} %bitcast.9, bf16[1,2048]{1,0:T(2,128)(2,1)} %broadcast_in_dim.11.mix, ...), custom_call_target="tpu_custom_call" | custom-call | tf_op jit(solution)/shard_map/pallas_call | solution.py:379
  56.7 1.4 %shard_map.212 = (bf16[8,2048]{1,0:T(8,128)(2,1)}, bf16[16,128]{1,0:T(8,128)(2,1)}, bf16[16,128]{1,0:T(8,128)(2,1)}) custom-call(bf16[8,2048]{1,0:T(8,128)(2,1)} %get-tuple-element.6.a, bf16[16,128]{1,0:T(8,128)(2,1)} %get-tuple-element.7.b, bf16[16,128]{1,0:T(8,128)(2,1)} %get-tuple-element.8.c), custom_call_target="tpu_custom_call" | custom-call | tf_op jit(solution)/shard_map/pallas_call | solution.py:394
